TPU v7x, 512 devices: a whole 4x4x16 slice. The times are simulated.
512 devices in a mesh: fs: 128 (over z, x, core), tp: 4 (over y).
Axes of the slice: x: 4, y: 4, z: 16, core: 2. Of those that a mesh axis runs over, the one named last changes fastest.
Arguments:
- tokens: bfloat16 [16384, 2048], P('fs', 'tp'), may hold values from -6 to 6
- routes: int32 [16384, 2], P('fs'), may hold values from 0 to 63, all different within a row; in each aligned block of 128 rows (0 to 127, 128 to 255, ...) at most 6 rows name the same one
- route_weight: float32 [16384, 2], P('fs'), may hold values from 0.1 to 1
- norm_gain: float32 [2048], P('fs'), may hold values from 0.1 to 1.9
- expert_gate: float32 [64, 2048, 512], P(None, 'fs', 'tp'), may hold values from -0.125 to 0.125
- expert_up: float32 [64, 2048, 512], P(None, 'fs', 'tp'), may hold values from -0.125 to 0.125
- expert_down: float32 [64, 2048, 512], P(None, 'fs', 'tp'), may hold values from -0.25 to 0.25
- shared_gate: float32 [2048, 512], P('fs', 'tp'), may hold values from -0.125 to 0.125
- shared_up: float32 [2048, 512], P('fs', 'tp'), may hold values from -0.125 to 0.125
- shared_down: float32 [512, 2048], P('tp', 'fs'), may hold values from -0.25 to 0.25
Outputs:
- mixed: bfloat16 [16384, 2048], P('fs', 'tp')
- gate_sampler: bfloat16 [128, 2048, 256], P('fs', None, 'tp')
- up_sampler: bfloat16 [128, 2048, 256], P('fs', None, 'tp')
- down_sampler: bfloat16 [128, 2048, 256], P('fs', 'tp')
- shared_gate_out: bfloat16 [2048, 512], P(None, 'tp')
- shared_up_out: bfloat16 [2048, 512], P(None, 'tp')
- shared_down_out: bfloat16 [512, 2048], P('tp')
Inputs may be any that keep to these rules, and one draw needn't show every extreme that they name: `routes`: each row names 2 different experts. In each aligned block of 128 rows no expert is named by more than 6 rows, a bound that some block reaches.
All inputs are finite; a program needn't handle non-finite values.
Results may differ from a plain program's by a relative error of at most 0.009.
Values may be sent and summed in bfloat16 or wider, within the bound.
A program may use at most 64 MiB of HBM per device.

v0:
```python
import jax
import jax.numpy as jnp
from jax import lax
from jax.sharding import Mesh
from jax.sharding import PartitionSpec as P

FS = ("fs_0", "fs_1", "fs_2")


EPS = 1e-06


def side_by_side(arrays, axis, split_dim, concat_dim, along):
    widths = [a.shape[along] for a in arrays]
    both = jnp.concatenate(arrays, axis=along)
    whole = lax.all_to_all(both, axis, split_axis=split_dim, concat_axis=concat_dim, tiled=True)
    return tuple(jnp.split(whole, [sum(widths[:k]) for k in range(1, len(widths))], axis=along))


def gather_turned(arrays, axis, dims):
    turned = [jnp.moveaxis(a, dim, 0) for a, dim in zip(arrays, dims)]
    both = jnp.concatenate([t.reshape(len(t), -1) for t in turned], axis=1)
    whole, at, finished = (lax.all_gather(both, axis, axis=0, tiled=True), 0, [])
    for t, dim in zip(turned, dims):
        slab = whole[:, at : at + t[0].size].reshape(-1, *t.shape[1:])
        finished.append(jnp.moveaxis(slab, 0, dim))
        at += t[0].size
    return tuple(finished)


def laid_out(pieces, dim):
    pieces = jnp.moveaxis(pieces, 0, dim)
    lengths = pieces.shape
    return pieces.reshape(*lengths[:dim], lengths[dim] * lengths[dim + 1], *lengths[dim + 2 :])


def sent_to_all(value, axis):
    peers = lax.axis_size(axis)
    return lax.all_to_all(
        jnp.broadcast_to(value[None], (peers, *value.shape)), axis, 0, 0, tiled=True
    )


def gather_directly(value, axis, dim):
    return laid_out(sent_to_all(value, axis), dim)


def split_up(value, dim, peers):
    before, after = (value.shape[:dim], value.shape[dim + 1 :])
    return jnp.moveaxis(value.reshape(*before, peers, -1, *after), dim, 0)


def sent_and_summed(value, axis, dim):
    pieces = split_up(value, dim, lax.axis_size(axis))
    arrived = lax.all_to_all(pieces, axis, split_axis=0, concat_axis=0, tiled=True)
    return arrived.astype(jnp.float32).sum(axis=0)


def turned_blocks(pieces, axes, sequence):
    lengths = [lax.axis_size(a) for a in axes]
    pieces = pieces.reshape(*lengths, *pieces.shape[1:])
    for k in sequence:
        pieces = lax.all_to_all(pieces, axes[k], split_axis=k, concat_axis=k, tiled=True)
    return pieces.reshape(-1, *pieces.shape[len(axes) :])


def core_and_chips(value, groups, sequence, split_dim, concat_dim):
    peers = lax.axis_size(groups[0]) * lax.axis_size(groups[1])
    pieces = split_up(value, split_dim, peers)
    return laid_out(turned_blocks(pieces, groups, sequence), concat_dim)


def to_owners(matrix, expert_count, unit_count):
    row_share = matrix.shape[1]
    return (
        matrix.reshape(expert_count, row_share, 2, unit_count)
        .transpose(0, 2, 1, 3)
        .reshape(2 * expert_count, row_share, unit_count)
    )


def on_device(
    tokens,
    routes,
    route_weight,
    norm_gain,
    expert_gate,
    expert_up,
    expert_down,
    shared_gate,
    shared_up,
    shared_down,
):
    fs_count = lax.axis_size(FS)
    tp_count = lax.axis_size("tp")
    expert_count, row_share, col_share = expert_gate.shape
    unit_count = col_share // 2
    model_width = row_share * fs_count
    quarter = model_width // tp_count
    tok_count, pick_count = routes.shape
    capacity = 2 * ((3 * tok_count * pick_count + 4 * expert_count - 1) // (4 * expert_count))
    slot_count = fs_count * capacity
    row_gain = norm_gain[None, :, None]
    gate_owned = to_owners((expert_gate * row_gain).astype(jnp.bfloat16), expert_count, unit_count)
    up_owned = to_owners((expert_up * row_gain).astype(jnp.bfloat16), expert_count, unit_count)
    gate_new, up_new = side_by_side((gate_owned, up_owned), FS, 0, 1, 2)
    down_owned = to_owners(expert_down.astype(jnp.bfloat16), expert_count, unit_count)
    down_new = lax.all_to_all(
        lax.all_to_all(down_owned, FS, split_axis=0, concat_axis=1, tiled=True),
        "tp",
        split_axis=1,
        concat_axis=2,
        tiled=True,
    )
    shared_gate_new, shared_up_new, shared_down_new = gather_turned(
        (
            (shared_gate * norm_gain[:, None]).astype(jnp.bfloat16),
            (shared_up * norm_gain[:, None]).astype(jnp.bfloat16),
            shared_down.astype(jnp.bfloat16),
        ),
        FS,
        (0, 0, 1),
    )
    gathered = gather_directly(tokens, "tp", 1)
    tokens_wide = gathered.astype(jnp.float32)
    normed = (
        tokens_wide * lax.rsqrt(jnp.mean(tokens_wide * tokens_wide, axis=1, keepdims=True) + EPS)
    ).astype(jnp.bfloat16)
    shared_act = jnp.dot(normed, shared_gate_new, preferred_element_type=jnp.float32)
    shared_lin = jnp.dot(normed, shared_up_new, preferred_element_type=jnp.float32)
    shared_hidden = (jax.nn.silu(shared_act) * shared_lin).astype(jnp.bfloat16)
    shared_term = jnp.dot(shared_hidden, shared_down_new, preferred_element_type=jnp.float32)
    shared_sum = sent_and_summed(shared_term.astype(jnp.bfloat16), "tp", 1)
    assigned = routes.reshape(-1)
    onehot = (assigned[:, None] == jnp.arange(expert_count, dtype=jnp.int32)[None, :]).astype(
        jnp.int32
    )
    earlier = jnp.cumsum(onehot, axis=0) - onehot
    position = jnp.sum(earlier * onehot, axis=1)
    slot_index = assigned * capacity + position
    token_index = jnp.arange(tok_count * pick_count, dtype=jnp.int32) // pick_count
    slot_token = (
        jnp.full((expert_count * capacity,), tok_count, jnp.int32).at[slot_index].set(token_index)
    )
    padded = jnp.concatenate([normed, jnp.zeros((1, model_width), jnp.bfloat16)], axis=0)
    own_part = lax.dynamic_slice_in_dim(padded, lax.axis_index("tp") * quarter, quarter, 1)
    outgoing = jnp.repeat(
        own_part[slot_token].reshape(expert_count, capacity, quarter), 2, axis=0
    ).reshape(slot_count, quarter)
    arrived = core_and_chips(outgoing, (("fs_0", "fs_1"), "fs_2"), (1, 0), 0, 0)
    portion = lax.all_gather(arrived, "tp", axis=1, tiled=True)
    gate_rows = gate_new[0]
    up_rows = up_new[0]
    gate_act = jnp.dot(portion, gate_rows, preferred_element_type=jnp.float32)
    up_act = jnp.dot(portion, up_rows, preferred_element_type=jnp.float32)
    hidden = (jax.nn.silu(gate_act) * up_act).astype(jnp.bfloat16)
    down_cols = down_new[0]
    half_sum = lax.dot_general(
        gather_directly(hidden, "tp", 1),
        down_cols,
        (((1,), (1,)), ((), ())),
        preferred_element_type=jnp.float32,
    )
    returned = lax.all_to_all(
        half_sum.astype(jnp.bfloat16), FS, split_axis=0, concat_axis=0, tiled=True
    )
    pair_sum = jnp.sum(
        returned.astype(jnp.float32).reshape(expert_count, 2, capacity, quarter), axis=1
    ).reshape(expert_count * capacity, quarter)
    gathered_slots = pair_sum[slot_index].reshape(tok_count, pick_count, quarter)
    routed = jnp.sum(gathered_slots * route_weight[:, :, None], axis=1)
    mixed = (shared_sum + routed).astype(jnp.bfloat16)
    return (mixed, gate_new, up_new, down_new, shared_gate_new, shared_up_new, shared_down_new)


def solution(mesh):
    split = Mesh(mesh.devices.reshape(16, 4, 2, mesh.shape["tp"]), ("fs_0", "fs_1", "fs_2", "tp"))
    placed = (
        P(FS, "tp"),
        P(FS, None),
        P(FS, None),
        P(FS),
        P(None, FS, "tp"),
        P(None, FS, "tp"),
        P(None, FS, "tp"),
        P(FS, "tp"),
        P(FS, "tp"),
        P("tp", FS),
    )
    return jax.shard_map(
        on_device,
        mesh=split,
        in_specs=placed,
        out_specs=(
            P(FS, "tp"),
            P(FS, None, "tp"),
            P(FS, None, "tp"),
            P(FS, "tp", None),
            P(None, "tp"),
            P(None, "tp"),
            P("tp", None),
        ),
        check_vma=False,
    )
```

profile of v0, /device:TPU:1, one launch (start us, length us, event | category | flops | bytes accessed | tf_op | source)
XLA Modules:
  0.0 320.2 jit_solution(2598705933041146886)
XLA Ops:
  7.2 1.7 broadcast_in_dim.10
  8.9 5.0 %all-to-all-start = ((bf16[4,128,512]{2,1,0:T(8,128)(2,1)}), bf16[4,128,512]{2,1,0:T(8,128)(2,1)S(1)}, u32[]{:S(2)}, u32[]{:S(2)}) async-start(bf16[4,128,512]{2,1,0:T(8,128)(2,1)} %broadcast_in_dim.10), calls=%async_computation | async-start | bytes 1048576 | tf_op jit(solution)/shard_map/all_to_all | solution.py:39
  19.1 1.4 scatter_custom_fusion
  21.4 2.1 gather_fusion
  23.8 10.4 %all_to_all.76 = bf16[64,2,6,512]{3,0,2,1:T(8,128)(2,1)S(1)} all-to-all(bf16[64,2,6,512]{3,0,2,1:T(8,128)(2,1)S(1)} %broadcast_in_dim.13), channel_id=1, replica_groups=mesh['fs_0'=16,'fs_1'=4,'fs_2'=2,'tp'=4] {'fs_2'}, dimensions={1} | all-to-all | bytes 1572864 | tf_op jit(solution)/shard_map/all_to_all | solution.py:63
  35.1 57.2 %all_to_all.77 = bf16[64,2,6,512]{3,1,2,0:T(2,128)(2,1)S(1)} all-to-all(bf16[64,2,6,512]{3,1,2,0:T(2,128)(2,1)S(1)} %copy.71), channel_id=1, replica_groups=mesh['fs_0'=16,'fs_1'=4,'fs_2'=2,'tp'=4] {'fs_0','fs_1'}, dimensions={0} | all-to-all | bytes 1572864 | tf_op jit(solution)/shard_map/all_to_all | solution.py:63
  92.5 1.2 reshape_reshape.3
  94.0 1.0 reshape.155
  95.0 10.0 %all-to-all-start.6 = ((bf16[128,2,512]{2,1,0:T(2,128)(2,1)}), bf16[128,2,512]{2,1,0:T(2,128)(2,1)S(1)}, u32[]{:S(2)}, u32[]{:S(2)}) async-start(bf16[128,2,512]{2,1,0:T(2,128)(2,1)} %reshape.155), calls=%async_computation.6 | async-start | bytes 524288 | tf_op jit(solution)/shard_map/all_to_all | solution.py:109
  105.7 1.1 pad_maximum_fusion.2
  106.8 18.9 %all-to-all-done.6 = bf16[128,2,512]{2,1,0:T(2,128)(2,1)S(1)} async-done(((bf16[128,2,512]{2,1,0:T(2,128)(2,1)}), bf16[128,2,512]{2,1,0:T(2,128)(2,1)S(1)}, u32[]{:S(2)}, u32[]{:S(2)}) %all-to-all-start.6) | async-done | bytes 262176 | tf_op jit(solution)/shard_map/all_to_all | solution.py:109
  125.7 8.9 %all-to-all-start.4 = ((bf16[128,16,128]{2,1,0:T(8,128)(2,1)}), bf16[128,16,128]{2,1,0:T(8,128)(2,1)S(1)}, u32[]{:S(2)}, u32[]{:S(2)}) async-start(bf16[128,16,128]{2,1,0:T(8,128)(2,1)} %pad_maximum_fusion.2), calls=%async_computation.4 | async-start | bytes 1048576 | tf_op jit(solution)/shard_map/all_to_all | solution.py:16
  134.9 8.1 %copy.89 = bf16[1,2048,64]{2,0,1:T(2,128)(2,1)S(1)} copy(bf16[1,2048,64]{2,1,0:T(8,128)(2,1)S(1)} %bitcast.80) | data formatting | bytes 524288 | tf_op jit(solution)/shard_map/all_to_all | solution.py:109
  143.5 11.5 %reduce.4 = bf16[2048,64]{1,0:T(8,128)(2,1)S(1)} reduce(bf16[2048,1,64]{2,1,0:T(2,128)(2,1)S(1)} %bitcast.75, bf16[]{:T(256)} %broadcast.94), dimensions={1}, to_apply=%bitcast.69.reduce_sub_computation | reduce | bytes 524290
  155.1 1.1 reshape.157
  156.2 13.0 %all-gather.3.cloned.1.call-done = bf16[2048,384]{1,0:T(8,128)(2,1)} async-done(((bf16[16,384]{1,0:T(8,128)(2,1)}), bf16[2048,384]{1,0:T(8,128)(2,1)}) %all-gather.3.cloned.1.call-update) | async-done | bytes 1572880 | tf_op jit(solution)/shard_map/all_gather | solution.py:23
  169.1 2.3 slice_bitcast_fusion
  171.4 3.6 %all-to-all-start.7 = ((bf16[4,2,16384]{2,1,0:T(2,128)(2,1)}), bf16[4,2,16384]{2,1,0:T(2,128)(2,1)S(1)}, u32[]{:S(2)}, u32[]{:S(2)}) async-start(bf16[4,2,16384]{2,1,0:T(2,128)(2,1)} %reshape.157), calls=%async_computation.7 | async-start | bytes 524288 | tf_op jit(solution)/shard_map/all_to_all | solution.py:108
  175.0 37.8 %all-gather.5.cloned.1.call-done = bf16[768,2048]{1,0:T(8,128)(2,1)} async-done(((bf16[768,512]{1,0:T(8,128)(2,1)}), bf16[768,2048]{1,0:T(8,128)(2,1)}) %all-gather.5.cloned.1.call-update) | async-done | bytes 3145744 | tf_op jit(solution)/shard_map/all_gather | solution.py:151
  212.8 3.1 fusion.4
  216.0 1.2 fusion
  217.9 3.5 %all-to-all-start.5 = ((bf16[4,768,64]{1,2,0:T(8,128)(2,1)}), bf16[4,768,64]{1,2,0:T(8,128)(2,1)S(1)}, u32[]{:S(2)}, u32[]{:S(2)}) async-start(bf16[4,768,64]{1,2,0:T(8,128)(2,1)} %broadcast_in_dim.14), calls=%async_computation.5 | async-start | bytes 786432 | tf_op jit(solution)/shard_map/all_to_all | solution.py:39
  221.7 1.6 convolution_convert_fusion
  224.1 4.3 %all-to-all-done.5 = bf16[4,768,64]{1,2,0:T(8,128)(2,1)S(1)} async-done(((bf16[4,768,64]{1,2,0:T(8,128)(2,1)}), bf16[4,768,64]{1,2,0:T(8,128)(2,1)S(1)}, u32[]{:S(2)}, u32[]{:S(2)}) %all-to-all-start.5) | async-done | bytes 393248 | tf_op jit(solution)/shard_map/all_to_all | solution.py:39
  228.4 3.5 %all-to-all-start.1 = ((bf16[4,128,512]{2,1,0:T(8,128)(2,1)}), bf16[4,128,512]{2,1,0:T(8,128)(2,1)S(1)}, u32[]{:S(2)}, u32[]{:S(2)}) async-start(bf16[4,128,512]{2,1,0:T(8,128)(2,1)} %bitcast.68), calls=%async_computation.1 | async-start | bytes 1048576 | tf_op jit(solution)/shard_map/all_to_all | solution.py:55
  233.8 1.2 all_to_all.64
  235.0 4.1 %all-to-all-done.1 = bf16[4,128,512]{2,1,0:T(8,128)(2,1)S(1)} async-done(((bf16[4,128,512]{2,1,0:T(8,128)(2,1)}), bf16[4,128,512]{2,1,0:T(8,128)(2,1)S(1)}, u32[]{:S(2)}, u32[]{:S(2)}) %all-to-all-start.1) | async-done | bytes 524320 | tf_op jit(solution)/shard_map/all_to_all | solution.py:55
  239.1 19.1 %all-to-all-start.8 = ((bf16[128,6,512]{2,1,0:T(8,128)(2,1)}), bf16[128,6,512]{2,1,0:T(8,128)(2,1)S(1)}, u32[]{:S(2)}, u32[]{:S(2)}) async-start(bf16[128,6,512]{2,1,0:T(8,128)(2,1)} %all_to_all.64), calls=%async_computation.8 | async-start | bytes 2097152 | tf_op jit(solution)/shard_map/all_to_all | solution.py:164
  259.2 1.0 fusion.22
  260.1 1.9 copy.78
  263.0 1.0 copy.81
  264.1 46.2 %all-to-all-done.8 = bf16[128,6,512]{2,1,0:T(8,128)(2,1)S(1)} async-done(((bf16[128,6,512]{2,1,0:T(8,128)(2,1)}), bf16[128,6,512]{2,1,0:T(8,128)(2,1)S(1)}, u32[]{:S(2)}, u32[]{:S(2)}) %all-to-all-start.8) | async-done | bytes 786464 | tf_op jit(solution)/shard_map/all_to_all | solution.py:164
  (83 shorter events, 17.9 us)
Async XLA Ops:
  8.9 11.9 %all-to-all-start = ((bf16[4,128,512]{2,1,0:T(8,128)(2,1)}), bf16[4,128,512]{2,1,0:T(8,128)(2,1)S(1)}, u32[]{:S(2)}, u32[]{:S(2)}) async-start(bf16[4,128,512]{2,1,0:T(8,128)(2,1)} %broadcast_in_dim.10), calls=%async_computation | async-start | bytes 1048576 | tf_op jit(solution)/shard_map/all_to_all | solution.py:39
  13.9 155.2 %all-gather.3.cloned.1.call-start = ((), (), s32[]{:S(2)}) async-start(), calls=%async_computation.9 | async-start | bytes 1585152 | tf_op jit(solution)/shard_map/all_gather | solution.py:23
  16.0 196.8 %all-gather.5.cloned.1.call-start = ((), (), s32[]{:S(2)}) async-start(), calls=%async_computation.10 | async-start | bytes 3932160 | tf_op jit(solution)/shard_map/all_gather | solution.py:151
  35.1 58.6 %copy-start.4 = (f32[64,16,128]{2,1,0:T(8,128)S(1)}, f32[64,16,128]{2,1,0:T(8,128)}, u32[]{:S(2)}) copy-start(f32[64,16,128]{2,1,0:T(8,128)} %param.16) | copy-start | bytes 1572868
  92.5 12.6 %copy-start.5 = (f32[64,16,128]{2,1,0:T(8,128)S(1)}, f32[64,16,128]{2,1,0:T(8,128)}, u32[]{:S(2)}) copy-start(f32[64,16,128]{2,1,0:T(8,128)} %param.14) | copy-start | bytes 1572868
  92.5 12.5 %copy-start.6 = (f32[64,16,128]{2,1,0:T(8,128)S(1)}, f32[64,16,128]{2,1,0:T(8,128)}, u32[]{:S(2)}) copy-start(f32[64,16,128]{2,1,0:T(8,128)} %param.15) | copy-start | bytes 1572868
  92.5 12.5 %copy-start.7 = (f32[16]{0:T(128)S(1)}, f32[16]{0:T(128)}, u32[]{:S(2)}) copy-start(f32[16]{0:T(128)} %param.13) | copy-start | bytes 196
  95.0 30.6 %all-to-all-start.6 = ((bf16[128,2,512]{2,1,0:T(2,128)(2,1)}), bf16[128,2,512]{2,1,0:T(2,128)(2,1)S(1)}, u32[]{:S(2)}, u32[]{:S(2)}) async-start(bf16[128,2,512]{2,1,0:T(2,128)(2,1)} %reshape.155), calls=%async_computation.6 | async-start | bytes 524288 | tf_op jit(solution)/shard_map/all_to_all | solution.py:109
  125.7 45.7 %all-to-all-start.4 = ((bf16[128,16,128]{2,1,0:T(8,128)(2,1)}), bf16[128,16,128]{2,1,0:T(8,128)(2,1)S(1)}, u32[]{:S(2)}, u32[]{:S(2)}) async-start(bf16[128,16,128]{2,1,0:T(8,128)(2,1)} %pad_maximum_fusion.2), calls=%async_computation.4 | async-start | bytes 1048576 | tf_op jit(solution)/shard_map/all_to_all | solution.py:16
  171.4 50.0 %copy-start.1 = (bf16[2048,128]{1,0:T(8,128)(2,1)}, bf16[2048,128]{1,0:T(8,128)(2,1)S(1)}, u32[]{:S(2)}) copy-start(bf16[2048,128]{1,0:T(8,128)(2,1)S(1)} %get-tuple-element.37) | copy-start | bytes 1572868
  171.4 50.3 %copy-start.3 = (bf16[2048,128]{1,0:T(8,128)(2,1)}, bf16[2048,128]{1,0:T(8,128)(2,1)S(1)}, u32[]{:S(2)}) copy-start(bf16[2048,128]{1,0:T(8,128)(2,1)S(1)} %get-tuple-element.36) | copy-start | bytes 1572868
  171.4 45.7 %all-to-all-start.7 = ((bf16[4,2,16384]{2,1,0:T(2,128)(2,1)}), bf16[4,2,16384]{2,1,0:T(2,128)(2,1)S(1)}, u32[]{:S(2)}, u32[]{:S(2)}) async-start(bf16[4,2,16384]{2,1,0:T(2,128)(2,1)} %reshape.157), calls=%async_computation.7 | async-start | bytes 524288 | tf_op jit(solution)/shard_map/all_to_all | solution.py:108
  212.8 3.1 copy-start
  217.9 10.5 %all-to-all-start.5 = ((bf16[4,768,64]{1,2,0:T(8,128)(2,1)}), bf16[4,768,64]{1,2,0:T(8,128)(2,1)S(1)}, u32[]{:S(2)}, u32[]{:S(2)}) async-start(bf16[4,768,64]{1,2,0:T(8,128)(2,1)} %broadcast_in_dim.14), calls=%async_computation.5 | async-start | bytes 786432 | tf_op jit(solution)/shard_map/all_to_all | solution.py:39
  228.4 10.7 %all-to-all-start.1 = ((bf16[4,128,512]{2,1,0:T(8,128)(2,1)}), bf16[4,128,512]{2,1,0:T(8,128)(2,1)S(1)}, u32[]{:S(2)}, u32[]{:S(2)}) async-start(bf16[4,128,512]{2,1,0:T(8,128)(2,1)} %bitcast.68), calls=%async_computation.1 | async-start | bytes 1048576 | tf_op jit(solution)/shard_map/all_to_all | solution.py:55
  233.1 25.1 %copy-start.8 = (f32[128,2]{0,1:T(2,128)S(1)}, f32[128,2]{0,1:T(2,128)}, u32[]{:S(2)}) copy-start(f32[128,2]{0,1:T(2,128)} %param.12) | copy-start | bytes 3076
  235.0 28.0 %copy-start.2 = (bf16[128,2048]{0,1:T(8,128)(2,1)S(1)}, bf16[128,2048]{0,1:T(8,128)(2,1)}, u32[]{:S(2)}) copy-start(bf16[128,2048]{0,1:T(8,128)(2,1)} %get-tuple-element.35) | copy-start | bytes 1572868
  239.1 71.2 %all-to-all-start.8 = ((bf16[128,6,512]{2,1,0:T(8,128)(2,1)}), bf16[128,6,512]{2,1,0:T(8,128)(2,1)S(1)}, u32[]{:S(2)}, u32[]{:S(2)}) async-start(bf16[128,6,512]{2,1,0:T(8,128)(2,1)} %all_to_all.64), calls=%async_computation.8 | async-start | bytes 2097152 | tf_op jit(solution)/shard_map/all_to_all | solution.py:164
Sparse Core Ops, SparseCore 0:
  18.3 150.7 all-gather.2
  171.2 41.5 all-gather.4
where the time goes:
time: 323 us; the launch traced here: 320 us
  waiting for transfers between devices  125 us (39%)
  blocking collectives  67.6 us (21%)
  starting transfers between devices  53.6 us (17%)
  local copies, waits for them, and re-layouts  34.6 us (11%)
  other arithmetic  18.9 us (6%)
  between operations  14.5 us (4%)
  matrix products  6.53 us (2%)
    all_to_all x2, blocking collectives, turned_blocks(): lax.all_to_all(pieces, axes[k], split_axis=k, concat_axis=k, tiled=True)  67.6 us
    all_to_all x1, waiting for transfers between devices, on_device(): lax.all_to_all(half_sum.astype(jnp.bfloat16), FS, split_axis=0, concat_ax...  46.2 us
    all_gather x1, waiting for transfers between devices, on_device(): portion = lax.all_gather(arrived, 'tp', axis=1, tiled=True)  37.8 us
    all_to_all x1, starting transfers between devices, on_device(): lax.all_to_all(half_sum.astype(jnp.bfloat16), FS, split_axis=0, concat_ax...  19.1 us
    all_to_all x1, waiting for transfers between devices, on_device(): lax.all_to_all(down_owned, FS, split_axis=0, concat_axis=1, tiled=True)  18.9 us
    all_gather x1, waiting for transfers between devices, gather_turned(): lax.all_gather(both, axis, axis=0, tiled=True)  13 us
    unnamed x2, other arithmetic  11.7 us
    all_to_all x1, starting transfers between devices, on_device(): lax.all_to_all(down_owned, FS, split_axis=0, concat_axis=1, tiled=True)  10 us
  transfers between devices with their start and end apart: 9, of which 7 were waited for; matrix products, arithmetic and copies ran while one was open for 17% of the time, Pallas kernels for 0%

commit v1 on v0

v1 whole, which is shorter than its diff:
```python
import functools

import jax
import jax.numpy as jnp
import numpy as np
from jax import lax
from jax.experimental import pallas as pl
from jax.experimental.pallas import tpu as pltpu
from jax.sharding import Mesh
from jax.sharding import PartitionSpec as P

FS = ("z", "x", "c")
EPS = 1e-06
MESH = pl.DeviceIdType.MESH
BF = jnp.bfloat16
F32 = jnp.float32
CAP = 6
LANES = 128


def turn_matrix():
    turn = np.zeros((8 * 4 * CAP, 8 * 4 * CAP), np.float32)
    for block in range(4):
        for source in range(8):
            for slot in range(CAP):
                turn[block * 8 * CAP + source * CAP + slot, source * 4 * CAP + block * CAP + slot] = 1
    return turn


def peer_at(step, z, x, zs, xs):
    pair = step // xs
    dz = pair // 2 + 1 - (zs // 2) * (pair % 2)
    dx = (step % xs + 1) % xs
    return lax.rem(z + dz + zs, zs), lax.rem(x + dx, xs)


def await_bytes(ref, sem):
    pltpu.make_async_copy(ref, ref, sem).wait()


def kernel(
    zs, xs, ys,
    tok, route, weight, gain, gate, up, down, s_gate, s_up, s_down, turn, turn_back,
    mixed, gate_out, up_out, down_out, sg_out, su_out, sd_out,
    tok_src, gu_src, down_src, tok_in, gu, down_in, dd, sh, own_tok, rows, normed, hid,
    part_src, part_in, back_src, back_in,
    send, recv, tok_sem, row_sem, hid_sem,
):
    z, x, c, y = (lax.axis_index(a) for a in ("z", "x", "c", "y"))
    me = z * xs + x
    others = zs * xs - 1
    above, below = lax.rem(y + 1, ys), lax.rem(y + ys - 1, ys)
    far = lax.rem(y + 2, ys)

    barrier = pltpu.get_barrier_semaphore()

    def greet(step, carry):
        pz, px = peer_at(step, z, x, zs, xs)
        pl.semaphore_signal(barrier, inc=1, device_id={"z": pz, "x": px}, device_id_type=MESH)
        return carry

    lax.fori_loop(0, others, greet, 0)
    for k in range(1, ys):
        pl.semaphore_signal(
            barrier, inc=1, device_id={"y": lax.rem(y + k, ys)}, device_id_type=MESH
        )
    pl.semaphore_signal(barrier, inc=1, device_id={"c": 1 - c}, device_id_type=MESH)

    experts = zs * xs
    slab = 4 * CAP
    shape = (experts, slab, LANES)
    expert_id = lax.broadcasted_iota(jnp.int32, shape, 0)
    place = lax.broadcasted_iota(jnp.int32, shape, 1)
    block = (
        (place >= CAP).astype(jnp.int32)
        + (place >= 2 * CAP).astype(jnp.int32)
        + (place >= 3 * CAP).astype(jnp.int32)
    )
    slot = place - CAP * block
    first = route[0:1, :].reshape(1, 1, LANES) == expert_id
    second = route[1:2, :].reshape(1, 1, LANES) == expert_id
    named = (first | second).astype(F32).reshape(experts * slab, LANES)
    before = (
        lax.broadcasted_iota(jnp.int32, (LANES, LANES), 0)
        < lax.broadcasted_iota(jnp.int32, (LANES, LANES), 1)
    ).astype(BF)
    position = jnp.dot(named.astype(BF), before, preferred_element_type=F32)
    slot_f = slot.astype(F32).reshape(experts * slab, LANES)
    picked = jnp.where(position == slot_f, named, 0.0)
    chosen = jnp.dot(picked.astype(BF), tok[...], preferred_element_type=F32)
    block_2d = block.reshape(experts * slab, LANES)
    packed = chosen[:, 0:LANES]
    for k in range(1, 4):
        packed = jnp.where(block_2d == k, chosen[:, k * LANES : (k + 1) * LANES], packed)
    tok_src[...] = packed.astype(BF).reshape(shape)
    scale = gain[...][None]
    gu_src[:, 0] = (gate[...] * scale).astype(BF)
    gu_src[:, 1] = (up[...] * scale).astype(BF)
    down_src[...] = down[...].astype(BF)
    sh[me, c, 0] = (s_gate[...] * gain[...]).astype(BF)
    sh[me, c, 1] = (s_up[...] * gain[...]).astype(BF)
    sh[me, c, 2] = s_down[...].astype(BF)
    own_tok[y] = tok[...]
    tok_in[me] = tok_src[me]
    gu[me, c] = gu_src[me]
    down_in[me] = down_src[me]

    pl.semaphore_wait(barrier, others + ys)

    def remote(src, dst, send_sem, recv_sem, to):
        return pltpu.make_async_remote_copy(
            src_ref=src, dst_ref=dst, send_sem=send_sem, recv_sem=recv_sem,
            device_id=to, device_id_type=MESH,
        )

    def ring_start(buf, sems):
        remote(buf.at[y], buf.at[y], sems.at[0], sems.at[4], {"y": above}).start()
        remote(buf.at[y], buf.at[y], sems.at[1], sems.at[5], {"y": below}).start()

    def ring_forward(buf, sems):
        half = buf.shape[1] // 2
        await_bytes(buf.at[below], sems.at[4])
        low = buf.at[below, pl.ds(0, half)]
        remote(low, low, sems.at[2], sems.at[6], {"y": above}).start()
        await_bytes(buf.at[above], sems.at[5])
        high = buf.at[above, pl.ds(half, half)]
        remote(high, high, sems.at[3], sems.at[7], {"y": below}).start()

    def ring_finish(buf, sems):
        half = buf.shape[1] // 2
        await_bytes(buf.at[far, pl.ds(0, half)], sems.at[6])
        await_bytes(buf.at[far, pl.ds(half, half)], sems.at[7])

    def ring_drain(buf, sems):
        half = buf.shape[1] // 2
        await_bytes(buf.at[y], sems.at[0])
        await_bytes(buf.at[y], sems.at[1])
        await_bytes(buf.at[y, pl.ds(0, half)], sems.at[2])
        await_bytes(buf.at[y, pl.ds(0, half)], sems.at[3])

    def to_columns(src_at, dst_at, number):
        def one(step, carry):
            pz, px = peer_at(step, z, x, zs, xs)
            remote(
                src_at(pz * xs + px), dst_at, send.at[number], recv.at[number],
                {"z": pz, "x": px},
            ).start()
            return carry

        lax.fori_loop(0, others, one, 0)

    quarter = zs // 4
    for k in range(1, 4):
        pz = lax.rem(z + k * quarter, zs)
        remote(sh.at[me, c], sh.at[me, c], send.at[0], recv.at[0], {"z": pz}).start()
    ring_start(own_tok, tok_sem)
    to_columns(lambda e: tok_src.at[e], tok_in.at[me], 1)
    await_bytes(sh.at[pl.ds(0, 3), c], recv.at[0])
    for k in range(1, quarter):
        pz = lax.rem(z - z % quarter + (z + k) % quarter, zs)
        for q in range(4):
            piece = (z % quarter + q * quarter) * xs + x
            remote(sh.at[piece, c], sh.at[piece, c], send.at[2], recv.at[2], {"z": pz}).start()
    to_columns(lambda e: gu_src.at[e], gu.at[me, c], 3)
    to_columns(lambda e: down_src.at[e], down_in.at[me], 4)
    ring_forward(own_tok, tok_sem)

    await_bytes(tok_in.at[pl.ds(0, others)], recv.at[1])
    group = 8 * CAP
    for g in range(experts // 8):
        lines = tok_in[pl.ds(8 * g, 8)].reshape(8 * slab, LANES)
        turned = jnp.dot(turn[...], lines, preferred_element_type=F32).astype(BF)
        for k in range(4):
            rows[y, pl.ds(g * group, group), pl.ds(k * LANES, LANES)] = turned[
                k * group : (k + 1) * group
            ]
    ring_start(rows, row_sem)

    await_bytes(sh.at[pl.ds(0, 4 * (quarter - 1)), c], recv.at[2])

    def spread(step, carry):
        piece = step * xs + x
        for k in range(1, xs):
            px = lax.rem(x + k, xs)
            remote(sh.at[piece, c], sh.at[piece, c], send.at[5], recv.at[5], {"x": px}).start()
        return carry

    lax.fori_loop(0, zs, spread, 0)

    ring_finish(own_tok, tok_sem)
    wide = [own_tok[k].astype(F32) for k in range(ys)]
    total = sum(jnp.sum(w * w, axis=1, keepdims=True) for w in wide)
    factor = lax.rsqrt(total * (1.0 / (ys * tok.shape[1])) + EPS)
    own_normed = [(w * factor).astype(BF) for w in wide]

    ring_forward(rows, row_sem)

    await_bytes(sh.at[pl.ds(0, (xs - 1) * zs), c], recv.at[5])
    remote(sh.at[:, c], sh.at[:, c], send.at[6], recv.at[6], {"c": 1 - c}).start()

    ring_finish(rows, row_sem)
    row_total = jnp.zeros((rows.shape[1], 1), F32)
    for k in range(ys):
        part = rows[k].astype(F32)
        row_total = row_total + jnp.sum(part * part, axis=1, keepdims=True)
    row_factor = lax.rsqrt(row_total * (1.0 / (ys * tok.shape[1])) + EPS)
    for k in range(ys):
        normed[k] = (rows[k].astype(F32) * row_factor).astype(BF)

    share = experts // ys
    await_bytes(sh.at[:, c], recv.at[6])

    def stacked(ref, k, number):
        return ref[pl.ds(k * share, share), :, number].reshape(share * 2 * 16, LANES)

    act = sum(
        jnp.dot(own_normed[k], stacked(sh, k, 0), preferred_element_type=F32) for k in range(ys)
    )
    lin = sum(
        jnp.dot(own_normed[k], stacked(sh, k, 1), preferred_element_type=F32) for k in range(ys)
    )
    shared_hidden = (act / (1.0 + jnp.exp(-act)) * lin).astype(BF)
    nt = (((1,), (1,)), ((), ()))
    for k in range(ys):
        part_src[k] = lax.dot_general(
            shared_hidden, stacked(sh, k, 2), nt, preferred_element_type=F32
        ).astype(BF)
    part_in[y] = part_src[y]
    for k in range(1, ys):
        to = lax.rem(y + k, ys)
        remote(part_src.at[to], part_in.at[y], send.at[7], recv.at[7], {"y": to}).start()

    await_bytes(gu.at[pl.ds(0, others), c], recv.at[3])
    remote(gu.at[:, c], gu.at[:, c], send.at[8], recv.at[8], {"c": 1 - c}).start()
    await_bytes(gu.at[:, c], recv.at[8])
    act = sum(
        jnp.dot(normed[k], stacked(gu, k, 0), preferred_element_type=F32) for k in range(ys)
    )
    lin = sum(
        jnp.dot(normed[k], stacked(gu, k, 1), preferred_element_type=F32) for k in range(ys)
    )
    hid[y] = (act / (1.0 + jnp.exp(-act)) * lin).astype(BF)
    ring_start(hid, hid_sem)

    await_bytes(down_in.at[pl.ds(0, others)], recv.at[4])
    dd[pl.ds(y * share, share), c] = down_in[pl.ds(y * share, share)]
    for k in range(1, ys):
        to = lax.rem(y + k, ys)
        remote(
            down_in.at[pl.ds(to * share, share)], dd.at[pl.ds(y * share, share), c],
            send.at[9], recv.at[9], {"y": to},
        ).start()
    ring_forward(hid, hid_sem)
    await_bytes(dd.at[pl.ds(0, (ys - 1) * share), c], recv.at[9])
    remote(dd.at[:, c], dd.at[:, c], send.at[10], recv.at[10], {"c": 1 - c}).start()
    ring_finish(hid, hid_sem)
    await_bytes(dd.at[:, c], recv.at[10])
    result = sum(
        lax.dot_general(
            hid[k], dd[pl.ds(k * share, share)].reshape(share * 2 * 16, LANES), nt,
            preferred_element_type=F32,
        )
        for k in range(ys)
    ).astype(BF)
    for g in range(experts // 8):
        part = result[g * group : (g + 1) * group]
        lines = jnp.concatenate([part[:, k * LANES : (k + 1) * LANES] for k in range(4)], axis=0)
        turned = jnp.dot(turn_back[...], lines, preferred_element_type=F32).astype(BF)
        back_src[pl.ds(8 * g, 8)] = turned.reshape(8, slab, LANES)
    back_in[me] = back_src[me]
    to_columns(lambda e: back_src.at[e], back_in.at[me], 11)

    half_rows = lax.broadcasted_iota(jnp.int32, (64, LANES), 0) + 64 * c
    pick = (half_rows == lax.broadcasted_iota(jnp.int32, (64, LANES), 1)).astype(BF)
    same = (
        lax.broadcasted_iota(jnp.int32, (LANES, LANES), 0)
        == lax.broadcasted_iota(jnp.int32, (LANES, LANES), 1)
    ).astype(BF)
    wide_share = share * 2 * 16
    for k in range(ys):
        cols = pl.ds(k * wide_share, wide_share)
        gate_out[0, :, cols] = lax.dot_general(
            pick, stacked(gu, k, 0), nt, preferred_element_type=F32
        ).astype(BF)
        up_out[0, :, cols] = lax.dot_general(
            pick, stacked(gu, k, 1), nt, preferred_element_type=F32
        ).astype(BF)
        sd_out[:, cols] = lax.dot_general(
            same, stacked(sh, k, 2), nt, preferred_element_type=F32
        ).astype(BF)
        sg_out[cols, :] = stacked(sh, k, 0)
        su_out[cols, :] = stacked(sh, k, 1)
    for k in range(ys // 2):
        left = dd[pl.ds(2 * k * share, share)].reshape(wide_share, LANES)
        right = dd[pl.ds((2 * k + 1) * share, share)].reshape(wide_share, LANES)
        left = lax.dot_general(left, pick, nt, preferred_element_type=F32)
        right = lax.dot_general(right, pick, nt, preferred_element_type=F32)
        down_out[0, :, pl.ds(k * LANES, LANES)] = jnp.concatenate([left, right], axis=1).astype(BF)

    await_bytes(part_in.at[pl.ds(0, ys - 1)], recv.at[7])
    shared_sum = sum(part_in[k].astype(F32) for k in range(ys))
    by_slot = jnp.where(first, weight[0:1, :].reshape(1, 1, LANES), 0.0) + jnp.where(
        second, weight[1:2, :].reshape(1, 1, LANES), 0.0
    )
    by_slot = jnp.where(position == slot_f, by_slot.reshape(experts * slab, LANES), 0.0)
    high = by_slot.astype(BF)
    low = (by_slot - high.astype(F32)).astype(BF)
    none = jnp.zeros_like(high)
    tn = (((0,), (0,)), ((), ()))
    await_bytes(back_in.at[pl.ds(0, others)], recv.at[11])
    arrived = back_in[...].reshape(experts * slab, LANES)
    for k in range(4):
        here = block_2d == k
        routed = lax.dot_general(
            jnp.where(here, high, none), arrived, tn, preferred_element_type=F32
        ) + lax.dot_general(jnp.where(here, low, none), arrived, tn, preferred_element_type=F32)
        lanes = slice(k * LANES, (k + 1) * LANES)
        mixed[:, lanes] = (shared_sum[:, lanes] + routed).astype(BF)

    await_bytes(sh.at[pl.ds(0, 3), c], send.at[0])
    await_bytes(tok_src.at[pl.ds(0, others)], send.at[1])
    await_bytes(sh.at[pl.ds(0, 4 * (quarter - 1)), c], send.at[2])
    await_bytes(gu_src.at[pl.ds(0, others)], send.at[3])
    await_bytes(down_src.at[pl.ds(0, others)], send.at[4])
    await_bytes(sh.at[pl.ds(0, (xs - 1) * zs), c], send.at[5])
    await_bytes(sh.at[:, c], send.at[6])
    await_bytes(part_src.at[pl.ds(0, ys - 1)], send.at[7])
    await_bytes(gu.at[:, c], send.at[8])
    await_bytes(down_in.at[pl.ds(0, (ys - 1) * share)], send.at[9])
    await_bytes(dd.at[:, c], send.at[10])
    await_bytes(back_src.at[pl.ds(0, others)], send.at[11])
    ring_drain(own_tok, tok_sem)
    ring_drain(rows, row_sem)
    ring_drain(hid, hid_sem)


def on_device(zs, xs, ys, tokens, routes, route_weight, norm_gain, e_gate, e_up, e_down, s_gate, s_up, s_down):
    experts, d_rows, _ = e_gate.shape
    tok_count, width = tokens.shape
    slab = 4 * CAP
    turn = turn_matrix()
    gain = jnp.broadcast_to(norm_gain[:, None], (d_rows, LANES))
    all_rows = experts * CAP
    model = experts * 2 * d_rows
    vmem = pl.BlockSpec(memory_space=pltpu.VMEM)
    outs = pl.pallas_call(
        functools.partial(kernel, zs, xs, ys),
        out_shape=(
            jax.ShapeDtypeStruct((tok_count, width), BF),
            jax.ShapeDtypeStruct((1, 64, model), BF),
            jax.ShapeDtypeStruct((1, 64, model), BF),
            jax.ShapeDtypeStruct((1, width, 2 * LANES), BF),
            jax.ShapeDtypeStruct((model, LANES), BF),
            jax.ShapeDtypeStruct((model, LANES), BF),
            jax.ShapeDtypeStruct((LANES, model), BF),
        ),
        in_specs=[vmem] * 12,
        out_specs=(vmem,) * 7,
        scratch_shapes=[
            pltpu.VMEM((experts, slab, LANES), BF),
            pltpu.VMEM((experts, 2, d_rows, LANES), BF),
            pltpu.VMEM((experts, d_rows, LANES), BF),
            pltpu.VMEM((experts, slab, LANES), BF),
            pltpu.VMEM((experts, 2, 2, d_rows, LANES), BF),
            pltpu.VMEM((experts, d_rows, LANES), BF),
            pltpu.VMEM((experts, 2, d_rows, LANES), BF),
            pltpu.VMEM((experts, 2, 3, d_rows, LANES), BF),
            pltpu.VMEM((ys, tok_count, width), BF),
            pltpu.VMEM((ys, all_rows, width), BF),
            pltpu.VMEM((ys, all_rows, width), BF),
            pltpu.VMEM((ys, all_rows, LANES), BF),
            pltpu.VMEM((ys, tok_count, width), BF),
            pltpu.VMEM((ys, tok_count, width), BF),
            pltpu.VMEM((experts, slab, LANES), BF),
            pltpu.VMEM((experts, slab, LANES), BF),
            pltpu.SemaphoreType.DMA((12,)),
            pltpu.SemaphoreType.DMA((12,)),
            pltpu.SemaphoreType.DMA((8,)),
            pltpu.SemaphoreType.DMA((8,)),
            pltpu.SemaphoreType.DMA((8,)),
        ],
        compiler_params=pltpu.CompilerParams(
            collective_id=0, has_side_effects=True, vmem_limit_bytes=44 * 1024 * 1024
        ),
    )(
        tokens, routes.T, route_weight.T, gain, e_gate, e_up, e_down, s_gate, s_up, s_down.T,
        jnp.asarray(turn, BF), jnp.asarray(turn.T, BF),
    )
    mixed, gate_t, up_t, down_new, sg, su, sd = outs
    return (
        mixed, gate_t.transpose(0, 2, 1), up_t.transpose(0, 2, 1), down_new, sg, su, sd,
    )


def solution(mesh):
    tp = mesh.shape["tp"]
    devices = mesh.devices.reshape(16, 4, 2, tp)
    split = Mesh(devices, ("z", "x", "c", "y"))
    zs, xs, _, ys = devices.shape
    placed = (
        P(FS, "y"),
        P(FS, None),
        P(FS, None),
        P(FS),
        P(None, FS, "y"),
        P(None, FS, "y"),
        P(None, FS, "y"),
        P(FS, "y"),
        P(FS, "y"),
        P("y", FS),
    )
    return jax.shard_map(
        functools.partial(on_device, zs, xs, ys),
        mesh=split,
        in_specs=placed,
        out_specs=(
            P(FS, "y"),
            P(FS, None, "y"),
            P(FS, None, "y"),
            P(FS, "y", None),
            P(None, "y"),
            P(None, "y"),
            P("y", None),
        ),
        check_vma=False,
    )
```

time: 323 us -> 131 us (0.41)
  waiting for transfers between devices: 125 us -> 0 us
  Pallas kernels: 0 us -> 116 us
  blocking collectives: 67.6 us -> 0 us
  starting transfers between devices: 53.6 us -> 0 us
  local copies, waits for them, and re-layouts: 34.6 us -> 13.1 us
  other arithmetic: 18.9 us -> 0 us
  between operations: 14.5 us -> 0.69 us
  matrix products: 6.53 us -> 0 us
    pallas_call x0 -> x1, Pallas kernels: none -> 116 us  [on_device(): pl.pallas_call(functools.partial(kernel, zs, xs, ys), out_shape=(jax.Shap...]
    all_to_all x7 -> x0, waiting for transfers between devices: 73.8 us -> none  [the longest x1 46.2 us: on_device(): lax.all_to_all(half_sum.astype(jnp.bfloat16), FS, split_axis=0, concat_ax...]
    all_to_all x2 -> x0, blocking collectives: 67.6 us -> none  [turned_blocks(): lax.all_to_all(pieces, axes[k], split_axis=k, concat_axis=k, tiled=True)]
    all_to_all x7 -> x0, starting transfers between devices: 53.5 us -> none  [the longest x1 19.1 us: on_device(): lax.all_to_all(half_sum.astype(jnp.bfloat16), FS, split_axis=0, concat_ax...]
    all_gather x2 -> x0, waiting for transfers between devices: 50.7 us -> none  [the longest x1 37.8 us: on_device(): portion = lax.all_gather(arrived, 'tp', axis=1, tiled=True)]
    unnamed x2 -> x0, other arithmetic: 11.7 us -> none
    all_to_all x7 -> x0, local copies, waits for them, and re-layouts: 11.2 us -> none  [the longest x1 8.14 us: on_device(): lax.all_to_all(down_owned, FS, split_axis=0, concat_axis=1, tiled=True)]
    dot_general x5 -> x0, matrix products: 6.53 us -> none  [the longest x1 3.12 us: on_device(): gate_act = jnp.dot(portion, gate_rows, preferred_element_type=jnp.float32)]
  transfers between devices with their start and end apart: 9 -> 0, of which waited for: 7 -> 0; matrix products, arithmetic and copies ran while one was open for 17% -> 0% of each run, Pallas kernels for 0% -> 0%
where the time goes in v1:
time: 131 us; the launch traced here: 130 us
  Pallas kernels  116 us (89%)
  local copies, waits for them, and re-layouts  13.1 us (10%)
    pallas_call x1, Pallas kernels, on_device(): pl.pallas_call(functools.partial(kernel, zs, xs, ys), out_shape=(jax.Shap...  116 us
    unnamed x29, local copies, waits for them, and re-layouts  12.4 us

profile of v1, /device:TPU:1, one launch (start us, length us, event | category | flops | bytes accessed | tf_op | source)
XLA Modules:
  0.0 130.3 jit_solution(3809356209685724940)
XLA Ops:
  0.6 0.0 copy-start.6
  0.6 0.0 copy-start.9
  0.7 0.0 copy-start.10
  0.7 0.7 broadcast_in_dim.2.gain
  1.4 0.0 copy-done.6
  1.4 0.0 copy-done.9
  1.4 0.0 copy-done.10
  1.4 0.0 copy-start
  1.4 1.0 copy-done
  2.5 0.0 copy-start.1
  2.5 1.0 copy-done.1
  3.5 0.0 copy-start.2
  3.5 1.0 copy-done.2
  4.5 0.0 copy-start.3
  4.5 0.9 copy-done.3
  5.5 0.0 copy-start.4
  5.5 0.9 copy-done.4
  6.3 0.0 copy-start.5
  6.3 0.9 copy-done.5
  7.2 0.0 copy-start.7
  7.2 0.7 copy-done.7
  7.9 0.0 copy-start.8
  7.9 0.7 copy-done.8
  8.6 116.5 %shard_map.171 = (bf16[128,512]{1,0:T(8,128)(2,1)S(1)}, bf16[1,64,2048]{2,1,0:T(8,128)(2,1)S(1)}, bf16[1,64,2048]{2,1,0:T(8,128)(2,1)S(1)}, bf16[1,512,256]{2,1,...) custom-call(bf16[128,512]{1,0:T(8,128)(2,1)S(1)} %copy-done.3, ...), custom_call_target="tpu_custom_call" | custom-call | tf_op jit(solution)/shard_map/pallas_call | solution.py:346
  125.1 0.7 copy.26
  125.8 0.7 copy.27
  126.5 0.7 copy.28
  127.2 0.7 copy.29
  127.9 0.8 copy.30
  128.7 0.8 copy.31
  129.5 0.8 copy.32
Async XLA Ops:
  0.6 0.8 copy-start.6
  0.6 0.8 copy-start.9
  0.7 0.8 copy-start.10
  1.4 1.0 copy-start
  2.5 1.0 copy-start.1
  3.5 1.0 copy-start.2
  4.5 0.9 copy-start.3
  5.5 0.9 copy-start.4
  6.3 0.9 copy-start.5
  7.2 0.7 copy-start.7
  7.9 0.7 copy-start.8

commit v2 on v1

v2 whole, which is shorter than its diff:
```python
import functools

import jax
import jax.numpy as jnp
import numpy as np
from jax import lax
from jax.experimental import pallas as pl
from jax.experimental.pallas import tpu as pltpu
from jax.sharding import Mesh
from jax.sharding import PartitionSpec as P

FS = ("z", "x", "c")
EPS = 1e-06
MESH = pl.DeviceIdType.MESH
BF = jnp.bfloat16
F32 = jnp.float32
CAP = 6
LANES = 128


def turn_matrix():
    turn = np.zeros((8 * 4 * CAP, 8 * 4 * CAP), np.float32)
    for block in range(4):
        for source in range(8):
            for slot in range(CAP):
                turn[block * 8 * CAP + source * CAP + slot, source * 4 * CAP + block * CAP + slot] = 1
    return turn


def peer_at(step, z, x, zs, xs):
    pair = step // xs
    dz = pair // 2 + 1 - (zs // 2) * (pair % 2)
    dx = (step % xs + 1) % xs
    return lax.rem(z + dz + zs, zs), lax.rem(x + dx, xs)


def await_bytes(ref, sem):
    pltpu.make_async_copy(ref, ref, sem).wait()


def kernel(
    zs, xs, ys,
    tok_hbm, route_hbm, weight_hbm, gain_hbm, gate_hbm, up_hbm, down_hbm, s_gate_hbm, s_up_hbm,
    s_down_hbm, turn_hbm, turn_back_hbm,
    mixed_hbm, gate_hbm_out, up_hbm_out, down_hbm_out, sg_hbm_out, su_hbm_out, sd_hbm_out,
    mixed, gate_out, up_out, down_out, sg_out, su_out, sd_out,
    tok_src, gu_src, down_src, tok_in, gu, dd, sh, own_tok, rows, normed, hid,
    part_src, part_in, result, back_src, back_in,
    tok, route, weight, gain, gate, up, down, s_gate, s_up, s_down, turn, turn_back,
    send, recv, row_sem, load_sem, store_sem,
):
    z, x, c, y = (lax.axis_index(a) for a in ("z", "x", "c", "y"))
    me = z * xs + x
    others = zs * xs - 1
    above, below = lax.rem(y + 1, ys), lax.rem(y + ys - 1, ys)
    far = lax.rem(y + 2, ys)

    loads = {}
    for number, (name, src, dst) in enumerate((
        ("route", route_hbm, route), ("tok", tok_hbm, tok), ("gain", gain_hbm, gain),
        ("gate", gate_hbm, gate), ("up", up_hbm, up), ("down", down_hbm, down),
        ("s_gate", s_gate_hbm, s_gate), ("s_up", s_up_hbm, s_up), ("s_down", s_down_hbm, s_down),
        ("weight", weight_hbm, weight), ("turn", turn_hbm, turn),
        ("turn_back", turn_back_hbm, turn_back),
    )):
        loads[name] = pltpu.make_async_copy(src, dst, load_sem.at[number])
        loads[name].start()

    barrier = pltpu.get_barrier_semaphore()

    def greet(step, carry):
        pz, px = peer_at(step, z, x, zs, xs)
        pl.semaphore_signal(barrier, inc=1, device_id={"z": pz, "x": px}, device_id_type=MESH)
        return carry

    lax.fori_loop(0, others, greet, 0)
    for k in range(1, ys):
        pl.semaphore_signal(
            barrier, inc=1, device_id={"y": lax.rem(y + k, ys)}, device_id_type=MESH
        )
    pl.semaphore_signal(barrier, inc=1, device_id={"c": 1 - c}, device_id_type=MESH)
    part_z = zs // ys
    owner = z // part_z

    def greet_sources(step, carry):
        pz = y * part_z + step // xs
        for k in range(1, ys):
            pl.semaphore_signal(
                barrier, inc=1,
                device_id={"z": pz, "x": lax.rem(step, xs), "y": lax.rem(y + k, ys)},
                device_id_type=MESH,
            )
        return carry

    lax.fori_loop(0, part_z * xs, greet_sources, 0)

    loads["route"].wait()
    loads["tok"].wait()
    experts = zs * xs
    slab = 4 * CAP
    shape = (experts, slab, LANES)
    expert_id = lax.broadcasted_iota(jnp.int32, shape, 0)
    place = lax.broadcasted_iota(jnp.int32, shape, 1)
    block = (
        (place >= CAP).astype(jnp.int32)
        + (place >= 2 * CAP).astype(jnp.int32)
        + (place >= 3 * CAP).astype(jnp.int32)
    )
    slot = place - CAP * block
    first = route[0:1, :].reshape(1, 1, LANES) == expert_id
    second = route[1:2, :].reshape(1, 1, LANES) == expert_id
    named = (first | second).astype(F32).reshape(experts * slab, LANES)
    before = (
        lax.broadcasted_iota(jnp.int32, (LANES, LANES), 0)
        < lax.broadcasted_iota(jnp.int32, (LANES, LANES), 1)
    ).astype(BF)
    position = jnp.dot(named.astype(BF), before, preferred_element_type=F32)
    slot_f = slot.astype(F32).reshape(experts * slab, LANES)
    picked = jnp.where(position == slot_f, named, 0.0)
    chosen = jnp.dot(picked.astype(BF), tok[...], preferred_element_type=F32)
    block_2d = block.reshape(experts * slab, LANES)
    packed = chosen[:, 0:LANES]
    for k in range(1, 4):
        packed = jnp.where(block_2d == k, chosen[:, k * LANES : (k + 1) * LANES], packed)
    tok_src[...] = packed.astype(BF).reshape(shape)
    loads["gain"].wait()
    rows_gain = jnp.sum(
        jnp.where(
            lax.broadcasted_iota(jnp.int32, (16, 16), 0)
            == lax.broadcasted_iota(jnp.int32, (16, 16), 1),
            jnp.broadcast_to(gain[...].reshape(1, 16), (16, 16)),
            0.0,
        ),
        axis=1,
        keepdims=True,
    )
    scale = rows_gain[None]
    for name in ("s_gate", "s_up", "s_down", "gate", "up", "down"):
        loads[name].wait()
    gu_src[:, 0] = (gate[...] * scale).astype(BF)
    gu_src[:, 1] = (up[...] * scale).astype(BF)
    down_src[...] = down[...].astype(BF)
    sh[z, x, c, 0] = (s_gate[...] * rows_gain).astype(BF)
    sh[z, x, c, 1] = (s_up[...] * rows_gain).astype(BF)
    sh[z, x, c, 2] = s_down[...].astype(BF)
    own_tok[y] = tok[...]
    tok_in[me] = tok_src[me]
    gu[me, c] = gu_src[me]

    for name in ("weight", "turn", "turn_back"):
        loads[name].wait()
    pl.semaphore_wait(barrier, others + ys + jnp.where(owner == y, 0, experts))

    def remote(src, dst, send_sem, recv_sem, to):
        return pltpu.make_async_remote_copy(
            src_ref=src, dst_ref=dst, send_sem=send_sem, recv_sem=recv_sem,
            device_id=to, device_id_type=MESH,
        )

    def ring_start(buf, sems):
        remote(buf.at[y], buf.at[y], sems.at[0], sems.at[4], {"y": above}).start()
        remote(buf.at[y], buf.at[y], sems.at[1], sems.at[5], {"y": below}).start()

    def ring_forward(buf, sems):
        half = buf.shape[1] // 2
        await_bytes(buf.at[below], sems.at[4])
        low = buf.at[below, pl.ds(0, half)]
        remote(low, low, sems.at[2], sems.at[6], {"y": above}).start()
        await_bytes(buf.at[above], sems.at[5])
        high = buf.at[above, pl.ds(half, half)]
        remote(high, high, sems.at[3], sems.at[7], {"y": below}).start()

    def ring_finish(buf, sems):
        half = buf.shape[1] // 2
        await_bytes(buf.at[far, pl.ds(0, half)], sems.at[6])
        await_bytes(buf.at[far, pl.ds(half, half)], sems.at[7])

    def ring_drain(buf, sems):
        half = buf.shape[1] // 2
        await_bytes(buf.at[y], sems.at[0])
        await_bytes(buf.at[y], sems.at[1])
        await_bytes(buf.at[y, pl.ds(0, half)], sems.at[2])
        await_bytes(buf.at[y, pl.ds(0, half)], sems.at[3])

    def spread_along_y(buf, number):
        for k in range(1, ys):
            to = lax.rem(y + k, ys)
            remote(buf.at[y], buf.at[y], send.at[number], recv.at[number], {"y": to}).start()

    def to_columns(src_at, dst_at, number, to_y=None):
        def one(step, carry):
            pz, px = peer_at(step, z, x, zs, xs)
            to = {"z": pz, "x": px}
            if to_y is not None:
                to["y"] = to_y
            remote(src_at(pz * xs + px), dst_at, send.at[number], recv.at[number], to).start()
            return carry

        lax.fori_loop(0, others, one, 0)

    quarter = zs // 4
    for k in range(1, 4):
        pz = lax.rem(z + k * quarter, zs)
        own = sh.at[z, x, c]
        remote(own, own, send.at[0], recv.at[0], {"z": pz}).start()
    spread_along_y(own_tok, 5)
    to_columns(lambda e: tok_src.at[e], tok_in.at[me], 1)
    to_columns(lambda e: gu_src.at[e], gu.at[me, c], 3)
    share = experts // ys
    down_at = dd.at[y * share + lax.rem(z, part_z) * xs + x, c]

    @pl.when(owner == y)
    def _():
        pltpu.make_async_copy(down_src.at[me], down_at, recv.at[4]).start()

    @pl.when(owner != y)
    def _():
        remote(down_src.at[me], down_at, send.at[9], recv.at[4], {"y": owner}).start()

    to_columns(lambda e: down_src.at[e], down_at, 4, owner)
    await_bytes(sh.at[pl.ds(0, 3), x, c], recv.at[0])
    for k in range(1, quarter):
        pz = lax.rem(z - z % quarter + (z + k) % quarter, zs)
        for q in range(4):
            piece = sh.at[z % quarter + q * quarter, x, c]
            remote(piece, piece, send.at[2], recv.at[2], {"z": pz}).start()

    await_bytes(tok_in.at[pl.ds(0, others)], recv.at[1])
    group = 8 * CAP
    for g in range(experts // 8):
        lines = tok_in[pl.ds(8 * g, 8)].reshape(8 * slab, LANES)
        turned = jnp.dot(turn[...], lines, preferred_element_type=F32).astype(BF)
        for k in range(4):
            rows[y, pl.ds(g * group, group), pl.ds(k * LANES, LANES)] = turned[
                k * group : (k + 1) * group
            ]
    ring_start(rows, row_sem)

    await_bytes(own_tok.at[pl.ds(0, ys - 1)], recv.at[5])
    wide = [own_tok[k].astype(F32) for k in range(ys)]
    total = sum(jnp.sum(w * w, axis=1, keepdims=True) for w in wide)
    factor = lax.rsqrt(total * (1.0 / (ys * tok.shape[1])) + EPS)
    own_normed = [(w * factor).astype(BF) for w in wide]

    ring_forward(rows, row_sem)

    ring_finish(rows, row_sem)
    row_total = jnp.zeros((rows.shape[1], 1), F32)
    for k in range(ys):
        part = rows[k].astype(F32)
        row_total = row_total + jnp.sum(part * part, axis=1, keepdims=True)
    row_factor = lax.rsqrt(row_total * (1.0 / (ys * tok.shape[1])) + EPS)
    for k in range(ys):
        normed[k] = (rows[k].astype(F32) * row_factor).astype(BF)

    nt = (((1,), (1,)), ((), ()))

    def shared_rows(k, number):
        return sh[pl.ds(k * part_z, part_z), :, :, number].reshape(share * 2 * 16, LANES)

    def stacked(ref, k, number):
        return ref[pl.ds(k * share, share), :, number].reshape(share * 2 * 16, LANES)

    await_bytes(gu.at[pl.ds(0, others), c], recv.at[3])
    remote(gu.at[:, c], gu.at[:, c], send.at[8], recv.at[8], {"c": 1 - c}).start()
    await_bytes(gu.at[:, c], recv.at[8])
    act = sum(
        jnp.dot(normed[k], stacked(gu, k, 0), preferred_element_type=F32) for k in range(ys)
    )
    lin = sum(
        jnp.dot(normed[k], stacked(gu, k, 1), preferred_element_type=F32) for k in range(ys)
    )
    hid[y] = (act / (1.0 + jnp.exp(-act)) * lin).astype(BF)
    spread_along_y(hid, 12)

    half_rows = lax.broadcasted_iota(jnp.int32, (64, LANES), 0) + 64 * c
    pick = (half_rows == lax.broadcasted_iota(jnp.int32, (64, LANES), 1)).astype(BF)
    wide_share = share * 2 * 16
    for k in range(ys):
        cols = pl.ds(k * wide_share, wide_share)
        gate_out[0, :, cols] = lax.dot_general(
            pick, stacked(gu, k, 0), nt, preferred_element_type=F32
        ).astype(BF)
        up_out[0, :, cols] = lax.dot_general(
            pick, stacked(gu, k, 1), nt, preferred_element_type=F32
        ).astype(BF)
    stores = [
        pltpu.make_async_copy(src, dst, store_sem.at[number])
        for number, (src, dst) in enumerate((
            (gate_out, gate_hbm_out), (up_out, up_hbm_out), (down_out, down_hbm_out),
            (sg_out, sg_hbm_out), (su_out, su_hbm_out), (sd_out, sd_hbm_out),
            (mixed, mixed_hbm),
        ))
    ]
    for store in stores[:2]:
        store.start()

    await_bytes(dd.at[:, c], recv.at[4])
    remote(dd.at[:, c], dd.at[:, c], send.at[10], recv.at[10], {"c": 1 - c}).start()
    await_bytes(hid.at[pl.ds(0, ys - 1)], recv.at[12])
    await_bytes(dd.at[:, c], recv.at[10])
    result[...] = sum(
        lax.dot_general(
            hid[k], dd[pl.ds(k * share, share)].reshape(wide_share, LANES), nt,
            preferred_element_type=F32,
        )
        for k in range(ys)
    ).astype(BF)

    await_bytes(sh.at[pl.ds(0, 4 * (quarter - 1)), x, c], recv.at[2])
    for k in range(1, xs):
        line = sh.at[:, x, c]
        remote(line, line, send.at[13], recv.at[13], {"x": lax.rem(x + k, xs)}).start()

    groups = experts // 8

    def send_back(g, count):
        def one(step, carry):
            pz = lax.rem(2 * g + (step // xs) + (z + 1) % 2, 2) + 2 * g
            px = lax.rem(x + 1 + lax.rem(step, xs), xs)
            remote(
                back_src.at[pz * xs + px], back_in.at[me], send.at[11], recv.at[11],
                {"z": pz, "x": px},
            ).start()
            return carry

        lax.fori_loop(0, count, one, 0)

    previous = None
    for offset in (4, 3, 5, 2, 6, 1, 7, 0):
        g = lax.rem(z // 2 + offset, groups)
        part = result[pl.ds(pl.multiple_of(g * group, 16), group), :]
        lines = jnp.concatenate([part[:, k * LANES : (k + 1) * LANES] for k in range(4)], axis=0)
        turned = jnp.dot(turn_back[...], lines, preferred_element_type=F32).astype(BF)
        back_src[pl.ds(8 * g, 8)] = turned.reshape(8, slab, LANES)
        if previous is not None:
            send_back(previous, 8)
        previous = g
    back_in[me] = back_src[me]
    send_back(previous, 7)

    for k in range(ys // 2):
        left = dd[pl.ds(2 * k * share, share)].reshape(wide_share, LANES)
        right = dd[pl.ds((2 * k + 1) * share, share)].reshape(wide_share, LANES)
        left = lax.dot_general(left, pick, nt, preferred_element_type=F32)
        right = lax.dot_general(right, pick, nt, preferred_element_type=F32)
        down_out[0, :, pl.ds(k * LANES, LANES)] = jnp.concatenate([left, right], axis=1).astype(BF)
    stores[2].start()
    await_bytes(sh.at[:, pl.ds(0, xs - 1), c], recv.at[13])
    half = sh.at[:, :, c]
    remote(half, half, send.at[6], recv.at[6], {"c": 1 - c}).start()
    await_bytes(half, recv.at[6])
    act = sum(
        jnp.dot(own_normed[k], shared_rows(k, 0), preferred_element_type=F32) for k in range(ys)
    )
    lin = sum(
        jnp.dot(own_normed[k], shared_rows(k, 1), preferred_element_type=F32) for k in range(ys)
    )
    shared_hidden = (act / (1.0 + jnp.exp(-act)) * lin).astype(BF)
    for k in range(ys):
        part_src[k] = lax.dot_general(
            shared_hidden, shared_rows(k, 2), nt, preferred_element_type=F32
        ).astype(BF)
    part_in[y] = part_src[y]
    for k in range(1, ys):
        to = lax.rem(y + k, ys)
        remote(part_src.at[to], part_in.at[y], send.at[7], recv.at[7], {"y": to}).start()

    same = (
        lax.broadcasted_iota(jnp.int32, (LANES, LANES), 0)
        == lax.broadcasted_iota(jnp.int32, (LANES, LANES), 1)
    ).astype(BF)
    for k in range(ys):
        cols = pl.ds(k * wide_share, wide_share)
        sd_out[:, cols] = lax.dot_general(
            same, shared_rows(k, 2), nt, preferred_element_type=F32
        ).astype(BF)
        sg_out[cols, :] = shared_rows(k, 0)
        su_out[cols, :] = shared_rows(k, 1)
    for store in stores[3:-1]:
        store.start()

    await_bytes(part_in.at[pl.ds(0, ys - 1)], recv.at[7])
    shared_sum = sum(part_in[k].astype(F32) for k in range(ys))
    by_slot = jnp.where(first, weight[0:1, :].reshape(1, 1, LANES), 0.0) + jnp.where(
        second, weight[1:2, :].reshape(1, 1, LANES), 0.0
    )
    by_slot = jnp.where(position == slot_f, by_slot.reshape(experts * slab, LANES), 0.0)
    high = by_slot.astype(BF)
    low = (by_slot - high.astype(F32)).astype(BF)
    none = jnp.zeros_like(high)
    tn = (((0,), (0,)), ((), ()))
    await_bytes(back_in.at[pl.ds(0, others)], recv.at[11])
    arrived = back_in[...].reshape(experts * slab, LANES)
    for k in range(4):
        here = block_2d == k
        routed = lax.dot_general(
            jnp.where(here, high, none), arrived, tn, preferred_element_type=F32
        ) + lax.dot_general(jnp.where(here, low, none), arrived, tn, preferred_element_type=F32)
        lanes = slice(k * LANES, (k + 1) * LANES)
        mixed[:, lanes] = (shared_sum[:, lanes] + routed).astype(BF)

    stores[-1].start()

    await_bytes(sh.at[pl.ds(0, 3), x, c], send.at[0])
    await_bytes(tok_src.at[pl.ds(0, others)], send.at[1])
    await_bytes(sh.at[pl.ds(0, 4 * (quarter - 1)), x, c], send.at[2])
    await_bytes(gu_src.at[pl.ds(0, others)], send.at[3])
    await_bytes(down_src.at[pl.ds(0, others)], send.at[4])
    await_bytes(own_tok.at[pl.ds(0, ys - 1)], send.at[5])
    await_bytes(hid.at[pl.ds(0, ys - 1)], send.at[12])
    await_bytes(sh.at[:, pl.ds(0, xs - 1), c], send.at[13])
    await_bytes(sh.at[:, :, c], send.at[6])
    await_bytes(part_src.at[pl.ds(0, ys - 1)], send.at[7])
    await_bytes(gu.at[:, c], send.at[8])

    @pl.when(owner != y)
    def _():
        await_bytes(down_src.at[me], send.at[9])

    await_bytes(dd.at[:, c], send.at[10])
    await_bytes(back_src.at[pl.ds(0, others)], send.at[11])
    ring_drain(rows, row_sem)
    for store in stores:
        store.wait()


def write_out(*refs):
    sources, targets, held, sems = refs[:7], refs[7:14], refs[14:21], refs[21]
    into = [pltpu.make_async_copy(sources[k], held[k], sems.at[k]) for k in range(7)]
    out = [pltpu.make_async_copy(held[k], targets[k], sems.at[7 + k]) for k in range(7)]
    for copy in into:
        copy.start()
    for k in range(7):
        into[k].wait()
        out[k].start()
    for copy in out:
        copy.wait()


def on_device(zs, xs, ys, tokens, routes, route_weight, norm_gain, e_gate, e_up, e_down, s_gate, s_up, s_down):
    experts, d_rows, _ = e_gate.shape
    tok_count, width = tokens.shape
    slab = 4 * CAP
    turn = turn_matrix()
    all_rows = experts * CAP
    model = experts * 2 * d_rows
    hbm = pl.BlockSpec(memory_space=pltpu.HBM)
    made = (
        ((tok_count, width), BF),
        ((1, 64, model), BF),
        ((1, 64, model), BF),
        ((1, width, 2 * LANES), BF),
        ((model, LANES), BF),
        ((model, LANES), BF),
        ((LANES, model), BF),
    )
    outs = pl.pallas_call(
        functools.partial(kernel, zs, xs, ys),
        out_shape=tuple(jax.ShapeDtypeStruct(*m) for m in made),
        in_specs=[hbm] * 12,
        out_specs=(hbm,) * 7,
        scratch_shapes=[pltpu.VMEM(*m) for m in made]
        + [
            pltpu.VMEM((experts, slab, LANES), BF),
            pltpu.VMEM((experts, 2, d_rows, LANES), BF),
            pltpu.VMEM((experts, d_rows, LANES), BF),
            pltpu.VMEM((experts, slab, LANES), BF),
            pltpu.VMEM((experts, 2, 2, d_rows, LANES), BF),
            pltpu.VMEM((experts, 2, d_rows, LANES), BF),
            pltpu.VMEM((zs, xs, 2, 3, d_rows, LANES), BF),
            pltpu.VMEM((ys, tok_count, width), BF),
            pltpu.VMEM((ys, all_rows, width), BF),
            pltpu.VMEM((ys, all_rows, width), BF),
            pltpu.VMEM((ys, all_rows, LANES), BF),
            pltpu.VMEM((ys, tok_count, width), BF),
            pltpu.VMEM((ys, tok_count, width), BF),
            pltpu.VMEM((all_rows, width), BF),
            pltpu.VMEM((experts, slab, LANES), BF),
            pltpu.VMEM((experts, slab, LANES), BF),
            pltpu.VMEM((tok_count, width), BF),
            pltpu.VMEM((2, LANES), jnp.int32),
            pltpu.VMEM((2, LANES), F32),
            pltpu.VMEM((d_rows,), F32),
            pltpu.VMEM((experts, d_rows, LANES), F32),
            pltpu.VMEM((experts, d_rows, LANES), F32),
            pltpu.VMEM((experts, d_rows, LANES), F32),
            pltpu.VMEM((d_rows, LANES), F32),
            pltpu.VMEM((d_rows, LANES), F32),
            pltpu.VMEM((d_rows, LANES), F32),
            pltpu.VMEM(turn.shape, BF),
            pltpu.VMEM(turn.shape, BF),
            pltpu.SemaphoreType.DMA((14,)),
            pltpu.SemaphoreType.DMA((14,)),
            pltpu.SemaphoreType.DMA((8,)),
            pltpu.SemaphoreType.DMA((12,)),
            pltpu.SemaphoreType.DMA((7,)),
        ],
        compiler_params=pltpu.CompilerParams(
            collective_id=0, has_side_effects=True, vmem_limit_bytes=61000 * 1024
        ),
    )(
        tokens, routes.T, route_weight.T, norm_gain, e_gate, e_up, e_down, s_gate, s_up, s_down.T,
        jnp.asarray(turn, BF), jnp.asarray(turn.T, BF),
    )
    mixed, gate_t, up_t, down_new, sg, su, sd = pl.pallas_call(
        write_out,
        out_shape=tuple(jax.ShapeDtypeStruct(o.shape, o.dtype) for o in outs),
        in_specs=[hbm] * 7,
        out_specs=(hbm,) * 7,
        scratch_shapes=[pltpu.VMEM(*m) for m in made] + [pltpu.SemaphoreType.DMA((14,))],
        compiler_params=pltpu.CompilerParams(vmem_limit_bytes=61000 * 1024),
    )(*outs)
    return (
        mixed, gate_t.transpose(0, 2, 1), up_t.transpose(0, 2, 1), down_new, sg, su, sd,
    )


def solution(mesh):
    tp = mesh.shape["tp"]
    devices = mesh.devices.reshape(16, 4, 2, tp)
    split = Mesh(devices, ("z", "x", "c", "y"))
    zs, xs, _, ys = devices.shape
    placed = (
        P(FS, "y"),
        P(FS, None),
        P(FS, None),
        P(FS),
        P(None, FS, "y"),
        P(None, FS, "y"),
        P(None, FS, "y"),
        P(FS, "y"),
        P(FS, "y"),
        P("y", FS),
    )
    return jax.shard_map(
        functools.partial(on_device, zs, xs, ys),
        mesh=split,
        in_specs=placed,
        out_specs=(
            P(FS, "y"),
            P(FS, None, "y"),
            P(FS, None, "y"),
            P(FS, "y", None),
            P(None, "y"),
            P(None, "y"),
            P("y", None),
        ),
        check_vma=False,
    )
```

time: 131 us -> 111 us (0.85); the launches traced: 130 us -> 109 us
  local copies, waits for them, and re-layouts: 13.1 us -> 0 us
  Pallas kernels: 116 us -> 108 us
    unnamed x29 -> x0, local copies, waits for them, and re-layouts: 12.4 us -> none
    pallas_call x1 -> x2, Pallas kernels: 116 us -> 108 us  [the longest x1 106 us: on_device(): pl.pallas_call(functools.partial(kernel, zs, xs, ys), out_shape=tuple((ja...]
where the time goes in v2:
time: 111 us; the launch traced here: 109 us
  Pallas kernels  108 us (97%)
    pallas_call x1, Pallas kernels, on_device(): pl.pallas_call(functools.partial(kernel, zs, xs, ys), out_shape=tuple((ja...  106 us
    pallas_call x1, Pallas kernels, on_device(): pl.pallas_call(write_out, out_shape=tuple((jax.ShapeDtypeStruct(o.shape,...  2.62 us

profile of v2, /device:TPU:1, one launch (start us, length us, event | category | flops | bytes accessed | tf_op | source)
XLA Modules:
  0.0 108.8 jit_solution(12655654837597550756)
XLA Ops:
  0.6 105.6 %shard_map.171 = (bf16[128,512]{1,0:T(8,128)(2,1)}, bf16[1,64,2048]{2,1,0:T(8,128)(2,1)}, bf16[1,64,2048]{2,1,0:T(8,128)(2,1)}, bf16[1,512,256]{2,1,0:T(8,128)(2...) custom-call(bf16[128,512]{1,0:T(8,128)(2,1)} %tok_hbm.1, s32[2,128]{1,0:T(2,128)} %bitcast.6, ...), custom_call_target="tpu_custom_call" | custom-call | tf_op jit(solution)/shard_map/pallas_call | solution.py:458
  106.2 2.6 %shard_map.172 = (bf16[128,512]{1,0:T(8,128)(2,1)}, bf16[1,64,2048]{2,1,0:T(8,128)(2,1)}, bf16[1,64,2048]{2,1,0:T(8,128)(2,1)}, bf16[1,512,256]{2,1,0:T(8,128)(2...) custom-call(bf16[128,512]{1,0:T(8,128)(2,1)} %get-tuple-element.21.refs_0_, ...), custom_call_target="tpu_custom_call" | custom-call | tf_op jit(solution)/shard_map/pallas_call | solution.py:506

commit v3 on v2

--- a/solution.py
+++ b/solution.py
@@ -51,9 +51,41 @@
 ):
     z, x, c, y = (lax.axis_index(a) for a in ("z", "x", "c", "y"))
     me = z * xs + x
+    fourth = zs // 4
+    q, r = z // fourth, z % fourth
     others = zs * xs - 1
     above, below = lax.rem(y + 1, ys), lax.rem(y + ys - 1, ys)
     far = lax.rem(y + 2, ys)
+
+    barrier = pltpu.get_barrier_semaphore()
+
+    def greet(step, carry):
+        pair = step // xs
+        dz = (zs // 2 - (pair + 1) // 2) * (2 * (pair % 2) - 1)
+        pz, px = lax.rem(z + dz + zs, zs), lax.rem(x + 1 + step % xs, xs)
+        pl.semaphore_signal(barrier, inc=1, device_id={"z": pz, "x": px}, device_id_type=MESH)
+        return carry
+
+    lax.fori_loop(0, others, greet, 0)
+    for k in range(1, ys):
+        pl.semaphore_signal(
+            barrier, inc=1, device_id={"y": lax.rem(y + k, ys)}, device_id_type=MESH
+        )
+    pl.semaphore_signal(barrier, inc=1, device_id={"c": 1 - c}, device_id_type=MESH)
+    part_z = zs // ys
+    owner = z // part_z
+
+    def greet_sources(step, carry):
+        pz = y * part_z + step // xs
+        for k in range(1, ys):
+            pl.semaphore_signal(
+                barrier, inc=1,
+                device_id={"z": pz, "x": lax.rem(step, xs), "y": lax.rem(y + k, ys)},
+                device_id_type=MESH,
+            )
+        return carry
+
+    lax.fori_loop(0, part_z * xs, greet_sources, 0)
 
     loads = {}
     for number, (name, src, dst) in enumerate((
@@ -65,34 +97,6 @@
     )):
         loads[name] = pltpu.make_async_copy(src, dst, load_sem.at[number])
         loads[name].start()
-
-    barrier = pltpu.get_barrier_semaphore()
-
-    def greet(step, carry):
-        pz, px = peer_at(step, z, x, zs, xs)
-        pl.semaphore_signal(barrier, inc=1, device_id={"z": pz, "x": px}, device_id_type=MESH)
-        return carry
-
-    lax.fori_loop(0, others, greet, 0)
-    for k in range(1, ys):
-        pl.semaphore_signal(
-            barrier, inc=1, device_id={"y": lax.rem(y + k, ys)}, device_id_type=MESH
-        )
-    pl.semaphore_signal(barrier, inc=1, device_id={"c": 1 - c}, device_id_type=MESH)
-    part_z = zs // ys
-    owner = z // part_z
-
-    def greet_sources(step, carry):
-        pz = y * part_z + step // xs
-        for k in range(1, ys):
-            pl.semaphore_signal(
-                barrier, inc=1,
-                device_id={"z": pz, "x": lax.rem(step, xs), "y": lax.rem(y + k, ys)},
-                device_id_type=MESH,
-            )
-        return carry
-
-    lax.fori_loop(0, part_z * xs, greet_sources, 0)
 
     loads["route"].wait()
     loads["tok"].wait()
@@ -140,9 +144,9 @@
     gu_src[:, 0] = (gate[...] * scale).astype(BF)
     gu_src[:, 1] = (up[...] * scale).astype(BF)
     down_src[...] = down[...].astype(BF)
-    sh[z, x, c, 0] = (s_gate[...] * rows_gain).astype(BF)
-    sh[z, x, c, 1] = (s_up[...] * rows_gain).astype(BF)
-    sh[z, x, c, 2] = s_down[...].astype(BF)
+    sh[q, r, x, c, 0] = (s_gate[...] * rows_gain).astype(BF)
+    sh[q, r, x, c, 1] = (s_up[...] * rows_gain).astype(BF)
+    sh[q, r, x, c, 2] = s_down[...].astype(BF)
     own_tok[y] = tok[...]
     tok_in[me] = tok_src[me]
     gu[me, c] = gu_src[me]
@@ -198,10 +202,9 @@
 
         lax.fori_loop(0, others, one, 0)
 
-    quarter = zs // 4
     for k in range(1, 4):
-        pz = lax.rem(z + k * quarter, zs)
-        own = sh.at[z, x, c]
+        pz = lax.rem(z + k * fourth, zs)
+        own = sh.at[q, r, x, c]
         remote(own, own, send.at[0], recv.at[0], {"z": pz}).start()
     spread_along_y(own_tok, 5)
     to_columns(lambda e: tok_src.at[e], tok_in.at[me], 1)
@@ -218,12 +221,13 @@
         remote(down_src.at[me], down_at, send.at[9], recv.at[4], {"y": owner}).start()
 
     to_columns(lambda e: down_src.at[e], down_at, 4, owner)
-    await_bytes(sh.at[pl.ds(0, 3), x, c], recv.at[0])
-    for k in range(1, quarter):
-        pz = lax.rem(z - z % quarter + (z + k) % quarter, zs)
-        for q in range(4):
-            piece = sh.at[z % quarter + q * quarter, x, c]
-            remote(piece, piece, send.at[2], recv.at[2], {"z": pz}).start()
+    await_bytes(sh.at[pl.ds(0, 3), r, x, c], recv.at[0])
+    line = sh.at[:, r, x, c]
+    for k in range(1, fourth):
+        pz = q * fourth + (r + k) % fourth
+        remote(line, line, send.at[2], recv.at[2], {"z": pz}).start()
+    for k in range(1, xs):
+        remote(line, line, send.at[14], recv.at[14], {"x": lax.rem(x + k, xs)}).start()
 
     await_bytes(tok_in.at[pl.ds(0, others)], recv.at[1])
     group = 8 * CAP
@@ -235,6 +239,9 @@
                 k * group : (k + 1) * group
             ]
     ring_start(rows, row_sem)
+    await_bytes(sh.at[:, r, pl.ds(0, xs - 1), c], recv.at[14])
+    first_lines = sh.at[:, r, :, c]
+    remote(first_lines, first_lines, send.at[6], recv.at[6], {"c": 1 - c}).start()
 
     await_bytes(own_tok.at[pl.ds(0, ys - 1)], recv.at[5])
     wide = [own_tok[k].astype(F32) for k in range(ys)]
@@ -256,7 +263,7 @@
     nt = (((1,), (1,)), ((), ()))
 
     def shared_rows(k, number):
-        return sh[pl.ds(k * part_z, part_z), :, :, number].reshape(share * 2 * 16, LANES)
+        return sh[k, :, :, :, number].reshape(share * 2 * 16, LANES)
 
     def stacked(ref, k, number):
         return ref[pl.ds(k * share, share), :, number].reshape(share * 2 * 16, LANES)
@@ -307,10 +314,19 @@
         for k in range(ys)
     ).astype(BF)
 
-    await_bytes(sh.at[pl.ds(0, 4 * (quarter - 1)), x, c], recv.at[2])
+    await_bytes(sh.at[:, pl.ds(0, fourth - 1), x, c], recv.at[2])
     for k in range(1, xs):
-        line = sh.at[:, x, c]
-        remote(line, line, send.at[13], recv.at[13], {"x": lax.rem(x + k, xs)}).start()
+        for j in range(1, fourth):
+            line = sh.at[:, (r + j) % fourth, x, c]
+            to = {"x": lax.rem(x + k, xs)}
+            remote(line, line, send.at[13], recv.at[14 + k], to).start()
+
+    def to_other_core(px):
+        for j in range(1, fourth):
+            line = sh.at[:, (r + j) % fourth, px, c]
+            remote(line, line, send.at[6], recv.at[6], {"c": 1 - c}).start()
+
+    to_other_core(x)
 
     groups = experts // 8
 
@@ -346,10 +362,10 @@
         right = lax.dot_general(right, pick, nt, preferred_element_type=F32)
         down_out[0, :, pl.ds(k * LANES, LANES)] = jnp.concatenate([left, right], axis=1).astype(BF)
     stores[2].start()
-    await_bytes(sh.at[:, pl.ds(0, xs - 1), c], recv.at[13])
-    half = sh.at[:, :, c]
-    remote(half, half, send.at[6], recv.at[6], {"c": 1 - c}).start()
-    await_bytes(half, recv.at[6])
+    for k in (1, 3, 2):
+        await_bytes(sh.at[:, pl.ds(0, fourth - 1), x, c], recv.at[14 + k])
+        to_other_core(lax.rem(x + xs - k, xs))
+    await_bytes(sh.at[:, :, :, c], recv.at[6])
     act = sum(
         jnp.dot(own_normed[k], shared_rows(k, 0), preferred_element_type=F32) for k in range(ys)
     )
@@ -402,15 +418,16 @@
 
     stores[-1].start()
 
-    await_bytes(sh.at[pl.ds(0, 3), x, c], send.at[0])
+    await_bytes(sh.at[pl.ds(0, 3), r, x, c], send.at[0])
     await_bytes(tok_src.at[pl.ds(0, others)], send.at[1])
-    await_bytes(sh.at[pl.ds(0, 4 * (quarter - 1)), x, c], send.at[2])
+    await_bytes(sh.at[:, pl.ds(0, fourth - 1), x, c], send.at[2])
+    await_bytes(sh.at[:, r, pl.ds(0, xs - 1), c], send.at[14])
     await_bytes(gu_src.at[pl.ds(0, others)], send.at[3])
     await_bytes(down_src.at[pl.ds(0, others)], send.at[4])
     await_bytes(own_tok.at[pl.ds(0, ys - 1)], send.at[5])
     await_bytes(hid.at[pl.ds(0, ys - 1)], send.at[12])
-    await_bytes(sh.at[:, pl.ds(0, xs - 1), c], send.at[13])
-    await_bytes(sh.at[:, :, c], send.at[6])
+    await_bytes(sh.at[:, pl.ds(0, fourth - 1), pl.ds(0, xs - 1), c], send.at[13])
+    await_bytes(sh.at[:, :, :, c], send.at[6])
     await_bytes(part_src.at[pl.ds(0, ys - 1)], send.at[7])
     await_bytes(gu.at[:, c], send.at[8])
 
@@ -468,7 +485,7 @@
             pltpu.VMEM((experts, slab, LANES), BF),
             pltpu.VMEM((experts, 2, 2, d_rows, LANES), BF),
             pltpu.VMEM((experts, 2, d_rows, LANES), BF),
-            pltpu.VMEM((zs, xs, 2, 3, d_rows, LANES), BF),
+            pltpu.VMEM((4, zs // 4, xs, 2, 3, d_rows, LANES), BF),
             pltpu.VMEM((ys, tok_count, width), BF),
             pltpu.VMEM((ys, all_rows, width), BF),
             pltpu.VMEM((ys, all_rows, width), BF),
@@ -490,8 +507,8 @@
             pltpu.VMEM((d_rows, LANES), F32),
             pltpu.VMEM(turn.shape, BF),
             pltpu.VMEM(turn.shape, BF),
-            pltpu.SemaphoreType.DMA((14,)),
-            pltpu.SemaphoreType.DMA((14,)),
+            pltpu.SemaphoreType.DMA((15,)),
+            pltpu.SemaphoreType.DMA((18,)),
             pltpu.SemaphoreType.DMA((8,)),
             pltpu.SemaphoreType.DMA((12,)),
             pltpu.SemaphoreType.DMA((7,)),

time: 111 us -> 107 us (0.964); the launches traced: 109 us -> 107 us
  Pallas kernels: 108 us -> 106 us
    pallas_call x1, Pallas kernels: 106 us -> 103 us  [on_device(): pl.pallas_call(functools.partial(kernel, zs, xs, ys), out_shape=tuple((ja...]
where the time goes in v3:
time: 107 us
  Pallas kernels  106 us (99%)
    pallas_call x1, Pallas kernels, on_device(): pl.pallas_call(functools.partial(kernel, zs, xs, ys), out_shape=tuple((ja...  103 us
    pallas_call x1, Pallas kernels, on_device(): pl.pallas_call(write_out, out_shape=tuple((jax.ShapeDtypeStruct(o.shape,...  2.62 us

profile of v3, /device:TPU:1, one launch (start us, length us, event | category | flops | bytes accessed | tf_op | source)
XLA Modules:
  0.0 106.7 jit_solution(5435667306208831418)
XLA Ops:
  0.6 103.4 %shard_map.171 = (bf16[128,512]{1,0:T(8,128)(2,1)}, bf16[1,64,2048]{2,1,0:T(8,128)(2,1)}, bf16[1,64,2048]{2,1,0:T(8,128)(2,1)}, bf16[1,512,256]{2,1,0:T(8,128)(2...) custom-call(bf16[128,512]{1,0:T(8,128)(2,1)} %tok_hbm.1, s32[2,128]{1,0:T(2,128)} %bitcast.6, ...), custom_call_target="tpu_custom_call" | custom-call | tf_op jit(solution)/shard_map/pallas_call | solution.py:475
  104.0 2.6 %shard_map.172 = (bf16[128,512]{1,0:T(8,128)(2,1)}, bf16[1,64,2048]{2,1,0:T(8,128)(2,1)}, bf16[1,64,2048]{2,1,0:T(8,128)(2,1)}, bf16[1,512,256]{2,1,0:T(8,128)(2...) custom-call(bf16[128,512]{1,0:T(8,128)(2,1)} %get-tuple-element.21.refs_0_, ...), custom_call_target="tpu_custom_call" | custom-call | tf_op jit(solution)/shard_map/pallas_call | solution.py:523
